TPU v7x, 128 devices: a whole 4x4x4 slice. The times are simulated.
128 devices in a mesh: fs: 16 (over z, y), tp: 8 (over x, core).
Axes of the slice: x: 4, y: 4, z: 4, core: 2. Of those that a mesh axis runs over, the one named last changes fastest.
Arguments:
- normed_input: bfloat16 [24576, 2048], P(('fs', 'tp')), may hold values from -6 to 6
- pre_act: bfloat16 [24576, 8192], P('fs', 'tp'), may hold values from -6 to 6
- out_grad: bfloat16 [24576, 2048], P(('fs', 'tp')), may hold values from -24 to 24
- up_weight: bfloat16 [2048, 8192], P('fs', 'tp'), may hold values from -0.125 to 0.125
- down_weight: bfloat16 [8192, 2048], P('tp', 'fs'), may hold values from -0.0625 to 0.0625
Outputs:
- input_grad: bfloat16 [24576, 2048], P(('fs', 'tp'))
- up_grad: float32 [2048, 8192], P('fs', 'tp')
- down_grad: float32 [8192, 2048], P('tp', 'fs')
All inputs are finite; a program needn't handle non-finite values.
Results may differ from a plain program's by a relative error of at most 0.014.
Values may be sent and summed in bfloat16 or wider, within the bound.
A program may use at most 128 MiB of HBM per device.

v0:
```python
import jax
import jax.numpy as jnp
from jax import lax
from jax.sharding import PartitionSpec as P


def sent_together(arrays, axis, dim, along):
    ends, at = ([], 0)
    for a in arrays[:-1]:
        at += a.shape[along]
        ends.append(at)
    both = jnp.concatenate(arrays, axis=along)
    return tuple(jnp.split(lax.all_gather(both, axis, axis=dim, tiled=True), ends, axis=along))


def cut_along(x, dim, count):
    before, after = (x.shape[:dim], x.shape[dim + 1 :])
    return jnp.moveaxis(x.reshape(*before, count, -1, *after), dim, 0)


def sum_at_owner(x, axis, dim):
    tiles = cut_along(x, dim, lax.axis_size(axis))
    arrived = lax.all_to_all(tiles, axis, split_axis=0, concat_axis=0, tiled=True)
    return arrived.astype(jnp.float32).sum(axis=0)


def local(normed_input, pre_act, out_grad, up_weight, down_weight):
    rows_all, grad_rows = sent_together((normed_input, out_grad), "tp", 0, 1)
    active = jnp.maximum(pre_act.astype(jnp.float32), 0.0)
    hidden = (active * active).astype(jnp.bfloat16)
    width = pre_act.shape[1]
    columns = grad_rows
    hidden_grad = jnp.dot(
        columns,
        lax.all_gather(down_weight, "fs", axis=1, tiled=True).T,
        preferred_element_type=jnp.float32,
    )
    pre_grad = (2.0 * active * hidden_grad).astype(jnp.bfloat16)
    partial_value = jnp.dot(
        pre_grad,
        lax.all_gather(up_weight, "fs", axis=0, tiled=True).T,
        preferred_element_type=jnp.float32,
    )
    rounded = lax.optimization_barrier(partial_value.astype(jnp.bfloat16))
    summed = sum_at_owner(rounded.astype(jnp.float32).astype(jnp.bfloat16), "tp", 0)
    input_grad = summed.astype(jnp.bfloat16)
    columns = rows_all
    both = lax.psum_scatter(
        jnp.concatenate(
            [
                jnp.dot(columns.T, pre_grad, preferred_element_type=jnp.float32),
                jnp.dot(grad_rows.T, hidden, preferred_element_type=jnp.float32),
            ],
            axis=1,
        ).astype(jnp.bfloat16),
        "fs",
        scatter_dimension=0,
        tiled=True,
    ).astype(jnp.float32)
    up_grad = both[:, :width]
    down_grad = both[:, width:].T
    up_grad, down_grad = (up_grad, down_grad)
    return (input_grad, up_grad, down_grad)


def solution(mesh):
    placed = (
        P(("fs", "tp"), None),
        P("fs", "tp"),
        P(("fs", "tp"), None),
        P("fs", "tp"),
        P("tp", "fs"),
    )
    return jax.shard_map(
        local,
        mesh=mesh,
        in_specs=placed,
        out_specs=(P(("fs", "tp"), None), P("fs", "tp"), P("tp", "fs")),
        check_vma=False,
    )
```

profile of v0, /device:TPU:1, one launch (start us, length us, event | category | flops | bytes accessed | tf_op | source)
XLA Modules:
  0.0 293.3 jit_solution(11470290909760394026)
XLA Ops:
  7.2 0.0 all-gather.4.cloned.1.call-start
  7.2 2.7 pad_maximum_fusion.1
  9.9 0.0 all-gather.6.cloned.1.call-start
  10.0 0.7 all-gather.6.cloned.1.call-update
  10.7 0.0 all-gather.8.cloned.1.call-start
  10.7 0.7 all-gather.8.cloned.1.call-update
  11.4 0.0 reduce-scatter.4.cloned.1.call-start
  11.5 69.5 %all-gather.4.cloned.1.call-done = bf16[1536,4096]{1,0:T(8,128)(2,1)} async-done(((bf16[192,4096]{1,0:T(8,128)(2,1)}), bf16[1536,4096]{1,0:T(8,128)(2,1)}) %all-gather.4.cloned.1.call-update) | async-done | bytes 12582928 | tf_op jit(solution)/shard_map/all_gather | solution.py:13
  80.9 11.6 %fusion.8 = bf16[2048,1024]{0,1:T(8,128)(2,1)} fusion(bf16[1536,4096]{1,0:T(8,128)(2,1)} %all-gather.4.cloned.1.call-done, bf16[1536,1024]{1,0:T(8,128)(2,1)} %param.6), kind=kOutput, calls=%fused_computation.11 | convolution fusion | flops 6450839552 | bytes 13631488 | tf_op jit(solution)/shard_map/dot_general | solution.py:52
  92.6 46.1 %all-gather.6.cloned.1.call-done = bf16[1024,2048]{1,0:T(8,128)(2,1)} async-done(((bf16[1024,128]{1,0:T(8,128)(2,1)}), bf16[1024,2048]{1,0:T(8,128)(2,1)}) %all-gather.6.cloned.1.call-update) | async-done | bytes 4194320 | tf_op jit(solution)/shard_map/all_gather | solution.py:35
  138.7 10.3 %multiply_convert_fusion.1 = bf16[1536,1024]{1,0:T(8,128)(2,1)S(1)} fusion(bf16[1536,1024]{1,0:T(8,128)(2,1)S(1)} %copy-done.1, bf16[1024,2048]{1,0:T(8,128)(2,1)} %all-gather.6.cloned.1.call-done, bf16[1536,4096]{1,0:T(8,128)(2,1)} %all-gather.4.cloned.1.call-done), kind=kOutput, calls=%fused_computation.5 | convolution fusion | flops 6450315264 | bytes 16777216 | tf_op jit(solution)/shard_map/dot_general | solution.py:33
  149.0 1.7 copy-done.2
  150.7 8.4 %fusion.11 = bf16[2048,1024]{0,1:T(8,128)(2,1)} fusion(bf16[1536,1024]{1,0:T(8,128)(2,1)S(1)} %multiply_convert_fusion.1, bf16[1536,4096]{1,0:T(8,128)(2,1)S(1)} %copy-done), kind=kOutput, calls=%fused_computation.12 | convolution fusion | flops 6444548096 | bytes 13631488 | tf_op jit(solution)/shard_map/dot_general | solution.py:51
  159.1 8.4 %pad_maximum_fusion = bf16[2048,2048]{0,1:T(8,128)(2,1)} fusion(bf16[2048,1024]{0,1:T(8,128)(2,1)} %fusion.8, bf16[2048,1024]{0,1:T(8,128)(2,1)} %fusion.11), kind=kLoop, calls=%fused_computation | loop fusion | flops 16777216 | bytes 16777216 | tf_op jit(solution)/shard_map/concatenate | solution.py:49
  167.5 11.9 %copy.10 = bf16[2048,2048]{1,0:T(8,128)(2,1)} copy(bf16[2048,2048]{0,1:T(8,128)(2,1)} %pad_maximum_fusion) | data formatting | bytes 16777216
  179.4 0.0 reduce-scatter.4.cloned.1.call-update
  179.4 13.4 %all-gather.8.cloned.1.call-done = bf16[2048,1024]{1,0:T(8,128)(2,1)} async-done(((bf16[128,1024]{1,0:T(8,128)(2,1)}), bf16[2048,1024]{1,0:T(8,128)(2,1)}) %all-gather.8.cloned.1.call-update) | async-done | bytes 4194320 | tf_op jit(solution)/shard_map/all_gather | solution.py:41
  192.8 9.3 %convolution_convert_fusion = bf16[1536,2048]{1,0:T(8,128)(2,1)S(1)} fusion(bf16[1536,1024]{1,0:T(8,128)(2,1)S(1)} %copy-done.3, bf16[2048,1024]{1,0:T(8,128)(2,1)} %all-gather.8.cloned.1.call-done), kind=kOutput, calls=%fused_computation.1 | convolution fusion | flops 6445596672 | bytes 13631488 | tf_op jit(solution)/shard_map/dot_general | solution.py:39
  202.2 76.1 %all_to_all.5 = bf16[8,192,2048]{2,1,0:T(8,128)(2,1)} all-to-all(bf16[8,192,2048]{2,1,0:T(8,128)(2,1)S(1)} %bitcast.8), channel_id=1, replica_groups=mesh['fs'=16,'tp'=8] {'tp'}, dimensions={0} | all-to-all | bytes 12582912 | tf_op jit(solution)/shard_map/all_to_all | solution.py:23
  278.3 5.2 %reduce_sum.12 = bf16[192,2048]{1,0:T(8,128)(2,1)} reduce(bf16[8,192,2048]{2,1,0:T(8,128)(2,1)} %all_to_all.5, bf16[]{:T(256)} %constant.6.clone.1), dimensions={0}, to_apply=%region_0.0 | reduce | flops 2752512 | bytes 7077890 | tf_op jit(solution)/shard_map/reduce_sum | solution.py:24
  283.5 1.3 copy.11
  284.8 0.1 convert_element_type.24
  284.9 0.8 slice_bitcast_fusion
  285.8 1.0 copy.9
  (10 shorter events, 0.1 us)
Async XLA Ops:
  7.2 73.8 %all-gather.4.cloned.1.call-start = ((), (), s32[]{:S(2)}) async-start(), calls=%async_computation.2 | async-start | bytes 14155776 | tf_op jit(solution)/shard_map/all_gather | solution.py:13
  9.9 128.8 %all-gather.6.cloned.1.call-start = ((), (), s32[]{:S(2)}) async-start(), calls=%async_computation.3 | async-start | bytes 4456448 | tf_op jit(solution)/shard_map/all_gather | solution.py:35
  10.7 182.1 %all-gather.8.cloned.1.call-start = ((), (), s32[]{:S(2)}) async-start(), calls=%async_computation.4 | async-start | bytes 4456448 | tf_op jit(solution)/shard_map/all_gather | solution.py:41
  11.4 127.3 %copy-start.1 = (bf16[1536,1024]{1,0:T(8,128)(2,1)S(1)}, bf16[1536,1024]{1,0:T(8,128)(2,1)}, u32[]{:S(2)}) copy-start(bf16[1536,1024]{1,0:T(8,128)(2,1)} %param.6) | copy-start | bytes 9437188
  11.4 272.0 %reduce-scatter.4.cloned.1.call-start = ((), (), s32[]{:S(2)}) async-start(), calls=%async_computation.5 | async-start | bytes 8912896
  138.7 12.0 %copy-start = (bf16[1536,4096]{1,0:T(8,128)(2,1)S(1)}, bf16[1536,4096]{1,0:T(8,128)(2,1)}, u32[]{:S(2)}) copy-start(bf16[1536,4096]{1,0:T(8,128)(2,1)} %all-gather.4.cloned.1.call-done) | copy-start | bytes 37748740
  149.0 1.7 copy-start.2
  179.4 13.4 %copy-start.3 = (bf16[1536,1024]{1,0:T(8,128)(2,1)S(1)}, bf16[1536,1024]{1,0:T(8,128)(2,1)}, u32[]{:S(2)}) copy-start(bf16[1536,1024]{1,0:T(8,128)(2,1)} %copy-done.2) | copy-start | bytes 9437188
Sparse Core Ops, SparseCore 0:
  10.1 70.8 all-gather.3
  83.0 55.6 all-gather.5
  140.8 51.9 all-gather.7
  196.1 84.5 reduce-scatter.3
where the time goes:
time: 294 us; the launch traced here: 293 us
  waiting for transfers between devices  130 us (44%)
  blocking collectives  76.1 us (26%)
  matrix products  39.6 us (13%)
  local copies, waits for them, and re-layouts  16.8 us (6%)
  other arithmetic  16.4 us (6%)
  between operations  13.8 us (5%)
    all_to_all x1, blocking collectives, sum_at_owner(): lax.all_to_all(tiles, axis, split_axis=0, concat_axis=0, tiled=True)  76.1 us
    all_gather x1, waiting for transfers between devices, sent_together(): lax.all_gather(both, axis, axis=dim, tiled=True)  69.5 us
    all_gather x1, waiting for transfers between devices, local(): lax.all_gather(down_weight, 'fs', axis=1, tiled=True)  46.1 us
    unnamed x11, local copies, waits for them, and re-layouts  15.9 us
    all_gather x1, waiting for transfers between devices, local(): lax.all_gather(up_weight, 'fs', axis=0, tiled=True)  13.4 us
    dot_general x1, matrix products, local(): jnp.dot(grad_rows.T, hidden, preferred_element_type=jnp.float32)  11.6 us
    dot_general x1, matrix products, local(): jnp.dot(columns, lax.all_gather(down_weight, 'fs', axis=1, tiled=True).T,...  10.3 us
    dot_general x1, matrix products, local(): jnp.dot(pre_grad, lax.all_gather(up_weight, 'fs', axis=0, tiled=True).T,...  9.33 us
  transfers between devices with their start and end apart: 4, of which 3 were waited for; matrix products, arithmetic and copies ran while one was open for 22% of the time, Pallas kernels for 0%

commit v1 on v0

--- a/solution.py
+++ b/solution.py
@@ -32,7 +32,12 @@
     columns = grad_rows
     hidden_grad = jnp.dot(
         columns,
-        lax.all_gather(down_weight, "fs", axis=1, tiled=True).T,
+        jnp.concatenate(
+            lax.all_to_all(
+                jnp.stack([down_weight for _ in range(lax.axis_size("fs"))]), "fs", 0, 0
+            ),
+            axis=1,
+        ).T,
         preferred_element_type=jnp.float32,
     )
     pre_grad = (2.0 * active * hidden_grad).astype(jnp.bfloat16)

time: 294 us -> 236 us (0.80)
  waiting for transfers between devices: 130 us -> 59 us
  starting transfers between devices: 0.16 us -> 8.75 us
  local copies, waits for them, and re-layouts: 16.8 us -> 22.4 us
    all_gather x1 -> x0, waiting for transfers between devices: 46.1 us -> none  [local(): lax.all_gather(down_weight, 'fs', axis=1, tiled=True)]
    all_gather x1, waiting for transfers between devices: 13.4 us -> 0.29 us  [local(): lax.all_gather(up_weight, 'fs', axis=0, tiled=True)]
    all_gather x1, waiting for transfers between devices: 69.5 us -> 57.9 us  [sent_together(): lax.all_gather(both, axis, axis=dim, tiled=True)]
    all_to_all x0 -> x1, starting transfers between devices: none -> 8.64 us  [local(): lax.all_to_all(jnp.stack([down_weight for _ in range(lax.axis_size('fs'))...]
    unnamed x11 -> x12, local copies, waits for them, and re-layouts: 15.9 us -> 19.1 us
  transfers between devices with their start and end apart: 4 -> 4, of which waited for: 3 -> 2; matrix products, arithmetic and copies ran while one was open for 22% -> 30% of each run, Pallas kernels for 0% -> 0%
where the time goes in v1:
time: 236 us; the launch traced here: 235 us
  blocking collectives  74.6 us (32%)
  waiting for transfers between devices  59 us (25%)
  matrix products  39.7 us (17%)
  local copies, waits for them, and re-layouts  22.4 us (9%)
  other arithmetic  16.7 us (7%)
  between operations  13.8 us (6%)
  starting transfers between devices  8.75 us (4%)
    all_to_all x1, blocking collectives, sum_at_owner(): lax.all_to_all(tiles, axis, split_axis=0, concat_axis=0, tiled=True)  74.6 us
    all_gather x1, waiting for transfers between devices, sent_together(): lax.all_gather(both, axis, axis=dim, tiled=True)  57.9 us
    unnamed x12, local copies, waits for them, and re-layouts  19.1 us
    dot_general x1, matrix products, local(): jnp.dot(grad_rows.T, hidden, preferred_element_type=jnp.float32)  11.2 us
    dot_general x1, matrix products, local(): jnp.dot(columns, jnp.concatenate(lax.all_to_all(jnp.stack([down_weight fo...  10.4 us
    dot_general x1, matrix products, local(): jnp.dot(pre_grad, lax.all_gather(up_weight, 'fs', axis=0, tiled=True).T,...  9.32 us
    dot_general x1, matrix products, local(): jnp.dot(columns.T, pre_grad, preferred_element_type=jnp.float32)  8.76 us
    concatenate x1, other arithmetic, local(): jnp.concatenate([jnp.dot(columns.T, pre_grad, preferred_element_type=jnp....  8.71 us
  transfers between devices with their start and end apart: 4, of which 2 were waited for; matrix products, arithmetic and copies ran while one was open for 30% of the time, Pallas kernels for 0%

profile of v1, /device:TPU:1, one launch (start us, length us, event | category | flops | bytes accessed | tf_op | source)
XLA Modules:
  0.0 235.0 jit_solution(5433989493618534094)
XLA Ops:
  7.2 0.0 all-gather.3.cloned.1.call-start
  7.2 2.7 %pad_maximum_fusion.1 = bf16[192,4096]{1,0:T(8,128)(2,1)} fusion(bf16[192,2048]{1,0:T(8,128)(2,1)} %param.7, bf16[192,2048]{1,0:T(8,128)(2,1)} %param.5), kind=kLoop, calls=%fused_computation.14 | loop fusion | flops 3145728 | bytes 3145728 | tf_op jit(solution)/shard_map/concatenate | solution.py:12
  9.9 1.1 copy.11
  11.0 2.5 %stack.2 = bf16[16,1024,128]{1,2,0:T(8,128)(2,1)} broadcast(bf16[1024,128]{0,1:T(8,128)(2,1)S(1)} %copy.11), dimensions={1,2} | broadcast | bytes 4456448 | tf_op jit(solution)/shard_map/stack | solution.py:37
  13.6 8.6 %all-to-all-start = ((bf16[16,1024,128]{1,2,0:T(8,128)(2,1)}), bf16[16,1024,128]{1,2,0:T(8,128)(2,1)}, u32[]{:S(2)}, u32[]{:S(2)}) async-start(bf16[16,1024,128]{1,2,0:T(8,128)(2,1)} %stack.2), calls=%async_computation | async-start | bytes 8388608 | tf_op jit(solution)/shard_map/all_to_all | solution.py:36
  22.2 0.0 all-gather.5.cloned.1.call-start
  22.2 0.7 all-gather.5.cloned.1.call-update
  23.0 0.0 reduce-scatter.4.cloned.1.call-start
  23.0 57.9 %all-gather.3.cloned.1.call-done = bf16[1536,4096]{1,0:T(8,128)(2,1)} async-done(((bf16[192,4096]{1,0:T(8,128)(2,1)}), bf16[1536,4096]{1,0:T(8,128)(2,1)}) %all-gather.3.cloned.1.call-update) | async-done | bytes 12582928 | tf_op jit(solution)/shard_map/all_gather | solution.py:13
  80.9 11.2 %fusion.8 = bf16[2048,1024]{0,1:T(8,128)(2,1)} fusion(bf16[1536,4096]{1,0:T(8,128)(2,1)} %all-gather.3.cloned.1.call-done, bf16[1536,1024]{1,0:T(8,128)(2,1)S(1)} %copy-done.1), kind=kOutput, calls=%fused_computation.11 | convolution fusion | flops 6450839552 | bytes 13631488 | tf_op jit(solution)/shard_map/dot_general | solution.py:57
  92.2 10.4 %multiply_convert_fusion.1 = bf16[1536,1024]{1,0:T(8,128)(2,1)S(1)} fusion(bf16[1536,1024]{1,0:T(8,128)(2,1)S(1)} %copy-done.1, bf16[1024,2048]{0,1:T(8,128)(2,1)} %bitcast.1, bf16[1536,4096]{1,0:T(8,128)(2,1)} %all-gather.3.cloned.1.call-done), kind=kOutput, calls=%fused_computation.5 | convolution fusion | flops 6450315264 | bytes 16777216 | tf_op jit(solution)/shard_map/dot_general | solution.py:33
  102.6 1.7 copy-done.2
  104.3 8.8 %fusion.11 = bf16[2048,1024]{0,1:T(8,128)(2,1)} fusion(bf16[1536,1024]{1,0:T(8,128)(2,1)S(1)} %multiply_convert_fusion.1, bf16[1536,4096]{1,0:T(8,128)(2,1)S(1)} %copy-done), kind=kOutput, calls=%fused_computation.12 | convolution fusion | flops 6444548096 | bytes 13631488 | tf_op jit(solution)/shard_map/dot_general | solution.py:56
  113.0 8.7 %pad_maximum_fusion = bf16[2048,2048]{0,1:T(8,128)(2,1)} fusion(bf16[2048,1024]{0,1:T(8,128)(2,1)} %fusion.8, bf16[2048,1024]{0,1:T(8,128)(2,1)} %fusion.11), kind=kLoop, calls=%fused_computation | loop fusion | flops 16777216 | bytes 16777216 | tf_op jit(solution)/shard_map/concatenate | solution.py:54
  121.8 12.4 %copy.13 = bf16[2048,2048]{1,0:T(8,128)(2,1)} copy(bf16[2048,2048]{0,1:T(8,128)(2,1)} %pad_maximum_fusion) | data formatting | bytes 16777216
  134.2 0.3 all-gather.5.cloned.1.call-done
  134.5 1.6 copy-done.3
  136.0 9.3 %convolution_convert_fusion = bf16[1536,2048]{1,0:T(8,128)(2,1)S(1)} fusion(bf16[1536,1024]{1,0:T(8,128)(2,1)S(1)} %copy-done.3, bf16[2048,1024]{1,0:T(8,128)(2,1)} %all-gather.5.cloned.1.call-done), kind=kOutput, calls=%fused_computation.1 | convolution fusion | flops 6445596672 | bytes 13631488 | tf_op jit(solution)/shard_map/dot_general | solution.py:44
  145.4 74.6 %all_to_all.10 = bf16[8,192,2048]{2,1,0:T(8,128)(2,1)} all-to-all(bf16[8,192,2048]{2,1,0:T(8,128)(2,1)S(1)} %bitcast.11), channel_id=1, replica_groups=mesh['fs'=16,'tp'=8] {'tp'}, dimensions={0} | all-to-all | bytes 12582912 | tf_op jit(solution)/shard_map/all_to_all | solution.py:23
  220.0 5.2 %reduce_sum.12 = bf16[192,2048]{1,0:T(8,128)(2,1)} reduce(bf16[8,192,2048]{2,1,0:T(8,128)(2,1)} %all_to_all.10, bf16[]{:T(256)} %constant.6.clone.1), dimensions={0}, to_apply=%region_0.0 | reduce | flops 2752512 | bytes 7077890 | tf_op jit(solution)/shard_map/reduce_sum | solution.py:24
  225.2 1.3 copy.14
  226.5 0.1 convert_element_type.24
  226.7 0.8 slice_bitcast_fusion
  227.5 1.0 copy.12
  (11 shorter events, 0.1 us)
Async XLA Ops:
  7.2 73.8 %all-gather.3.cloned.1.call-start = ((), (), s32[]{:S(2)}) async-start(), calls=%async_computation.3 | async-start | bytes 14155776 | tf_op jit(solution)/shard_map/all_gather | solution.py:13
  11.0 69.9 %copy-start.1 = (bf16[1536,1024]{1,0:T(8,128)(2,1)S(1)}, bf16[1536,1024]{1,0:T(8,128)(2,1)}, u32[]{:S(2)}) copy-start(bf16[1536,1024]{1,0:T(8,128)(2,1)} %param.6) | copy-start | bytes 9437188
  13.6 78.6 %all-to-all-start = ((bf16[16,1024,128]{1,2,0:T(8,128)(2,1)}), bf16[16,1024,128]{1,2,0:T(8,128)(2,1)}, u32[]{:S(2)}, u32[]{:S(2)}) async-start(bf16[16,1024,128]{1,2,0:T(8,128)(2,1)} %stack.2), calls=%async_computation | async-start | bytes 8388608 | tf_op jit(solution)/shard_map/all_to_all | solution.py:36
  22.2 112.3 %all-gather.5.cloned.1.call-start = ((), (), s32[]{:S(2)}) async-start(), calls=%async_computation.4 | async-start | bytes 4456448 | tf_op jit(solution)/shard_map/all_gather | solution.py:46
  23.0 202.3 %reduce-scatter.4.cloned.1.call-start = ((), (), s32[]{:S(2)}) async-start(), calls=%async_computation.5 | async-start | bytes 8912896
  92.2 12.1 %copy-start = (bf16[1536,4096]{1,0:T(8,128)(2,1)S(1)}, bf16[1536,4096]{1,0:T(8,128)(2,1)}, u32[]{:S(2)}) copy-start(bf16[1536,4096]{1,0:T(8,128)(2,1)} %all-gather.3.cloned.1.call-done) | copy-start | bytes 37748740
  102.6 1.7 copy-start.2
  134.1 1.9 copy-start.3
Sparse Core Ops, SparseCore 0:
  10.1 70.8 all-gather.2
  83.1 51.3 all-gather.4
  137.9 84.4 reduce-scatter.3
